TPU v7x, 32 devices: a whole 2x2x4 slice. The times are simulated.
32 devices in a mesh: fs: 4 (over z), rep: 4 (over y, x), tp: 2 (over core).
Axes of the slice: x: 2, y: 2, z: 4, core: 2. Of those that a mesh axis runs over, the one named last changes fastest.
Arguments:
- mixer_out: bfloat16 [16384, 1536], P(('fs', 'rep')), may hold values from -6 to 6
- out_grad: bfloat16 [16384, 4096], P(('fs', 'rep'), 'tp'), may hold values from -0.046875 to 0.046875
- factors: bfloat16 [1536, 256], P(('fs', 'rep')), may hold values from -0.15625 to 0.15625
- weight: float32 [1536, 4096], P(('fs', 'rep'), 'tp'), may hold values from -0.15625 to 0.15625
- first_moment: float32 [256, 4096], P(('fs', 'rep'), 'tp'), may hold values from -6 to 6
- second_moment: float32 [256, 4096], P(('fs', 'rep'), 'tp'), may hold values from 0.05 to 2
Outputs:
- new_weight: float32 [1536, 4096], P(('fs', 'rep'), 'tp')
- update: float32 [1536, 4096], P(('fs', 'rep'), 'tp')
- new_first: float32 [256, 4096], P(('fs', 'rep'), 'tp')
- new_second: float32 [256, 4096], P(('fs', 'rep'), 'tp')
- weight_copy: bfloat16 [1536, 4096], P(None, 'tp')
All inputs are finite; a program needn't handle non-finite values.
Results may differ from a plain program's by a relative error of at most 0.0034.
Values may be sent and summed in bfloat16 or wider, within the bound.
A program may use at most 64 MiB of HBM per device.

v0:
```python
import jax
import jax.numpy as jnp
from jax import lax
from jax.sharding import PartitionSpec as P


def contract_rows(left, right):
    return lax.dot_general(
        left, right, (((0,), (0,)), ((), ())), preferred_element_type=jnp.float32
    )


def per_device(mixer_out, out_grad, factors, weight, first_moment, second_moment):
    columns = mixer_out
    gradient = lax.psum_scatter(
        contract_rows(columns, out_grad), ("fs", "rep"), scatter_dimension=0, tiled=True
    )
    grad_low = gradient.astype(jnp.bfloat16)
    columns = factors
    projected = lax.psum_scatter(
        contract_rows(columns, grad_low), ("fs", "rep"), scatter_dimension=0, tiled=True
    )
    new_first = 0.8 * first_moment + 0.2 * projected
    new_second = 0.9 * second_moment + 0.1 * projected * projected
    direction = new_first / (jnp.sqrt(new_second) + 1e-08)
    dir_low = direction.astype(jnp.bfloat16)
    proj_low = projected.astype(jnp.bfloat16)
    dir_whole, proj_whole = (
        lax.all_gather(dir_low, ("fs", "rep"), axis=0, tiled=True),
        lax.all_gather(proj_low, ("fs", "rep"), axis=0, tiled=True),
    )
    dir_wide = dir_low.astype(jnp.float32)
    proj_wide = proj_low.astype(jnp.float32)
    dir_sum, proj_sum = lax.psum(
        (jnp.sum(dir_wide * dir_wide), jnp.sum(proj_wide * proj_wide)), ("fs", "rep", "tp")
    )
    back_dir = jnp.dot(factors, dir_whole, preferred_element_type=jnp.float32)
    back_proj = jnp.dot(factors, proj_whole, preferred_element_type=jnp.float32)
    scale_ratio = jnp.sqrt(dir_sum) / jnp.sqrt(proj_sum + 1e-06)
    update = back_dir + scale_ratio * (gradient - back_proj)
    new_weight = weight - 0.01 * update
    weight_copy = lax.all_gather(new_weight.astype(jnp.bfloat16), ("fs", "rep"), axis=0, tiled=True)
    return (new_weight, update, new_first, new_second, weight_copy)


def solution(mesh):
    in_specs = (
        P(("fs", "rep"), None),
        P(("fs", "rep"), "tp"),
        P(("fs", "rep"), None),
        P(("fs", "rep"), "tp"),
        P(("fs", "rep"), "tp"),
        P(("fs", "rep"), "tp"),
    )
    out_specs = (
        P(("fs", "rep"), "tp"),
        P(("fs", "rep"), "tp"),
        P(("fs", "rep"), "tp"),
        P(("fs", "rep"), "tp"),
        P(None, "tp"),
    )
    return jax.shard_map(
        per_device, mesh=mesh, in_specs=in_specs, out_specs=out_specs, check_vma=False
    )
```

profile of v0, /device:TPU:18, one launch (start us, length us, event | category | flops | bytes accessed | tf_op | source)
XLA Modules:
  0.0 531.8 jit_solution(9787667784067138825)
XLA Ops:
  7.2 0.0 copy-start
  7.2 0.0 reduce-scatter.5.cloned.1.call-start
  7.2 1.8 copy-done
  9.1 11.3 %fusion.7 = f32[1536,2048]{1,0:T(8,128)} fusion(bf16[1024,1536]{1,0:T(8,128)(2,1)S(1)} %copy-done, bf16[1024,2048]{1,0:T(8,128)(2,1)} %param.7), kind=kOutput, calls=%fused_computation.15 | convolution fusion | flops 6442450944 | bytes 19922944 | tf_op jit(solution)/shard_map/dot_general | solution.py:8
  20.4 0.0 copy-start.1
  20.4 0.0 reduce-scatter.5.cloned.1.call-update
  20.4 0.0 copy-start.2
  20.4 0.0 copy-start.3
  20.4 0.0 reduce-scatter.7.cloned.1.call-start
  20.5 203.4 %reduce-scatter.5.cloned.1.call-done = f32[96,2048]{1,0:T(8,128)} async-done(((f32[1536,2048]{1,0:T(8,128)}), f32[96,2048]{1,0:T(8,128)}) %reduce-scatter.5.cloned.1.call-update) | async-done | bytes 786448 | tf_op jit(solution)/shard_map/reduce_scatter | solution.py:15
  223.8 0.0 copy-done.1
  223.8 2.9 convolution_bitcast_fusion
  226.8 2.9 copy.29
  229.7 0.0 reduce-scatter.7.cloned.1.call-update
  229.7 0.0 all-gather.6.cloned.1.call-start
  229.8 70.9 %reduce-scatter.7.cloned.1.call-done = f32[16,2048]{1,0:T(8,128)} async-done(((f32[256,2048]{1,0:T(8,128)}), f32[16,2048]{1,0:T(8,128)}) %reduce-scatter.7.cloned.1.call-update) | async-done | bytes 131088 | tf_op jit(solution)/shard_map/reduce_scatter | solution.py:20
  300.7 0.0 copy-done.2
  300.7 0.0 copy-done.3
  300.7 2.4 multiply_reduce_fusion.1
  303.1 0.0 all-gather.6.cloned.1.call-update
  303.1 0.0 all-gather.4.cloned.1.call-start
  303.2 0.5 all-gather.4.cloned.1.call-update
  303.7 0.0 all-gather.8.cloned.1.call-start
  303.7 49.1 %all-reduce = (f32[]{:T(128)}, f32[]{:T(128)}) all-reduce(f32[]{:T(128)} %get-tuple-element.21, f32[]{:T(128)} %get-tuple-element.25), channel_id=1, replica_groups=mesh['fs'=4,'rep'=4,'tp'=2] {'fs','rep','tp'}, use_global_device_ids=true, to_apply=%region_3.0 | all-reduce | flops 2 | bytes 16 | tf_op jit(solution)/shard_map/psum | solution.py:34
  354.3 10.3 %all-gather.6.cloned.1.call-done = bf16[256,2048]{1,0:T(8,128)(2,1)} async-done(((bf16[16,2048]{1,0:T(8,128)(2,1)}), bf16[256,2048]{1,0:T(8,128)(2,1)}) %all-gather.6.cloned.1.call-update) | async-done | bytes 1048592 | tf_op jit(solution)/shard_map/all_gather | solution.py:30
  364.6 2.6 fusion.2
  367.2 54.5 %all-gather.4.cloned.1.call-done = bf16[256,2048]{1,0:T(8,128)(2,1)} async-done(((bf16[16,2048]{1,0:T(8,128)(2,1)}), bf16[256,2048]{1,0:T(8,128)(2,1)}) %all-gather.4.cloned.1.call-update) | async-done | bytes 1048592 | tf_op jit(solution)/shard_map/all_gather | solution.py:29
  421.7 3.3 fusion.5
  425.0 0.0 all-gather.8.cloned.1.call-update
  425.0 93.6 %all-gather.8.cloned.1.call-done = bf16[1536,2048]{1,0:T(8,128)(2,1)} async-done(((bf16[96,2048]{1,0:T(8,128)(2,1)}), bf16[1536,2048]{1,0:T(8,128)(2,1)}) %all-gather.8.cloned.1.call-update) | async-done | bytes 6291472 | tf_op jit(solution)/shard_map/all_gather | solution.py:42
  518.6 6.6 %copy.32 = bf16[1536,2048]{1,0:T(8,128)(2,1)} copy(bf16[1536,2048]{1,0:T(8,128)(2,1)} %all-gather.8.cloned.1.call-done) | data formatting | bytes 12582912
Async XLA Ops:
  7.2 1.9 copy-start
  7.2 216.6 %reduce-scatter.5.cloned.1.call-start = ((), (), s32[]{:S(2)}) async-start(), calls=%async_computation.2 | async-start | bytes 13369344 | tf_op jit(solution)/shard_map/reduce_scatter | solution.py:15
  20.4 203.5 %copy-start.1 = (bf16[96,256]{1,0:T(8,128)(2,1)S(1)}, bf16[96,256]{1,0:T(8,128)(2,1)}, u32[]{:S(2)}) copy-start(bf16[96,256]{1,0:T(8,128)(2,1)} %param.8) | copy-start | bytes 147460
  20.4 280.3 %copy-start.2 = (f32[16,2048]{1,0:T(8,128)S(1)}, f32[16,2048]{1,0:T(8,128)}, u32[]{:S(2)}) copy-start(f32[16,2048]{1,0:T(8,128)} %param.11) | copy-start | bytes 393220
  20.4 280.3 %copy-start.3 = (f32[16,2048]{1,0:T(8,128)S(1)}, f32[16,2048]{1,0:T(8,128)}, u32[]{:S(2)}) copy-start(f32[16,2048]{1,0:T(8,128)} %param.10) | copy-start | bytes 393220
  20.4 280.3 %reduce-scatter.7.cloned.1.call-start = ((), (), s32[]{:S(2)}) async-start(), calls=%async_computation.6 | async-start | bytes 2228224 | tf_op jit(solution)/shard_map/reduce_scatter | solution.py:20
  229.7 134.8 %all-gather.6.cloned.1.call-start = ((), (), s32[]{:S(2)}) async-start(), calls=%async_computation.4 | async-start | bytes 1114112 | tf_op jit(solution)/shard_map/all_gather | solution.py:30
  303.1 118.6 %all-gather.4.cloned.1.call-start = ((), (), s32[]{:S(2)}) async-start(), calls=%async_computation.3 | async-start | bytes 1114112 | tf_op jit(solution)/shard_map/all_gather | solution.py:29
  303.7 214.9 %all-gather.8.cloned.1.call-start = ((), (), s32[]{:S(2)}) async-start(), calls=%async_computation.5 | async-start | bytes 6684672 | tf_op jit(solution)/shard_map/all_gather | solution.py:42
Sparse Core Ops, SparseCore 0:
  20.5 203.2 reduce-scatter.4
  229.8 70.8 reduce-scatter.6
  304.0 60.4 all-gather.5
  367.7 53.9 all-gather.3
  425.1 93.4 all-gather.7
where the time goes:
time: 534 us; the launch traced here: 532 us
  waiting for transfers between devices  433 us (81%)
  blocking collectives  49.1 us (9%)
  matrix products  20.1 us (4%)
  between operations  15.2 us (3%)
  local copies, waits for them, and re-layouts  11.4 us (2%)
    reduce_scatter x1, waiting for transfers between devices, per_device(): lax.psum_scatter(contract_rows(columns, out_grad), ('fs', 'rep'), scatter...  203 us
    all_gather x1, waiting for transfers between devices, per_device(): lax.all_gather(new_weight.astype(jnp.bfloat16), ('fs', 'rep'), axis=0, ti...  93.6 us
    reduce_scatter x1, waiting for transfers between devices, per_device(): lax.psum_scatter(contract_rows(columns, grad_low), ('fs', 'rep'), scatter...  70.9 us
    all_gather x1, waiting for transfers between devices, per_device(): lax.all_gather(dir_low, ('fs', 'rep'), axis=0, tiled=True)  54.5 us
    psum x1, blocking collectives, per_device(): lax.psum((jnp.sum(dir_wide * dir_wide), jnp.sum(proj_wide * proj_wide)),...  49.1 us
    dot_general x2, matrix products, contract_rows(): lax.dot_general(left, right, (((0,), (0,)), ((), ())), preferred_element_...  14.2 us
    unnamed x10, local copies, waits for them, and re-layouts  11.4 us
  transfers between devices with their start and end apart: 5, of which 5 were waited for; matrix products, arithmetic and copies ran while one was open for 0% of the time, Pallas kernels for 0%

commit v1 on v0

--- a/solution.py
+++ b/solution.py
@@ -1,7 +1,15 @@
+import functools
+
 import jax
 import jax.numpy as jnp
 from jax import lax
+from jax.experimental import pallas as pl
+from jax.experimental.pallas import tpu as pltpu
 from jax.sharding import PartitionSpec as P
+
+MESH = pl.DeviceIdType.MESH
+LANES = 128
+TILE = 256
 
 
 def contract_rows(left, right):
@@ -10,7 +18,378 @@
     )
 
 
-def per_device(mixer_out, out_grad, factors, weight, first_moment, second_moment):
+def fused_kernel(
+    Z, R, T,
+    m_ref, o_ref, f_ref, w_ref, m1_ref, m2_ref,
+    nw_ref, upd_ref, nf_ref, ns_ref, wc_ref,
+    mt, send1, recv1, own, send2, recv2, grad, f_all, m1_all, m2_all,
+    nf_col, ns_col, upd_col, stat, stat_all,
+    s1_send, s1_recv, s2_send, s2_recv,
+    fa_send, fa_recv, ma_send, ma_recv, mb_send, mb_recv,
+    st_send, st_recv, nf_send, nf_recv, ns_send, ns_recv, up_send, up_recv,
+    gz_send, gz_recv, gr_send, gr_recv,
+):
+    N = Z * R
+    z, r, t = lax.axis_index("fs"), lax.axis_index("rep"), lax.axis_index("tp")
+    me = z * R + r
+    every = me * T + t
+    DH = m_ref.shape[1]
+    FR = f_ref.shape[0]
+    MR = m1_ref.shape[0]
+
+    def device(zz, rr, tt):
+        return {"fs": zz, "rep": rr, "tp": tt}
+
+    def peer(p):
+        q = lax.rem(me + p, N)
+        return q, q // R, lax.rem(q, R)
+
+    def column(zz, rr):
+        return pl.ds(pl.multiple_of((rr * Z + zz) * LANES, LANES), LANES)
+
+    def rows(q, size):
+        return pl.ds(pl.multiple_of(q * size, size), size)
+
+    barrier = pltpu.get_barrier_semaphore()
+
+    def greet(p, carry):
+        q = lax.rem(every + p, N * T)
+        d = q // T
+        pl.semaphore_signal(
+            barrier, inc=1, device_id=device(d // R, lax.rem(d, R), lax.rem(q, T)), device_id_type=MESH
+        )
+        return carry
+
+    lax.fori_loop(1, N * T, greet, 0)
+
+    def turn(i, carry):
+        part = pl.ds(pl.multiple_of(i * TILE, TILE), TILE)
+        mt[part, :] = m_ref[:, part].T
+        return carry
+
+    lax.fori_loop(0, DH // TILE, turn, 0)
+    pl.semaphore_wait(barrier, N * T - 1)
+
+    def product(zz, rr, store):
+        cols = column(zz, rr)
+
+        def tile(i, carry):
+            part = pl.ds(pl.multiple_of(i * TILE, TILE), TILE)
+            store(part, jnp.dot(mt[part, :], o_ref[:, cols], preferred_element_type=jnp.float32))
+            return carry
+
+        lax.fori_loop(0, DH // TILE, tile, 0)
+
+    def first(rr, zz, src):
+        return pltpu.make_async_remote_copy(
+            src_ref=send1.at[rr, zz], dst_ref=recv1.at[src, zz],
+            send_sem=s1_send.at[rr, zz], recv_sem=s1_recv.at[src, zz],
+            device_id=device(z, rr, t), device_id_type=MESH,
+        )
+
+    def second(zz, src):
+        return pltpu.make_async_remote_copy(
+            src_ref=send2.at[zz], dst_ref=recv2.at[src],
+            send_sem=s2_send.at[zz], recv_sem=s2_recv.at[src],
+            device_id=device(zz, r, t), device_id_type=MESH,
+        )
+
+    def phase1(i, carry):
+        zz = lax.rem(z + 1 + i // (R - 1), Z)
+        rr = lax.rem(r + 1 + lax.rem(i, R - 1), R)
+
+        def store(part, value):
+            send1[rr, zz, part, :] = value.astype(jnp.bfloat16)
+
+        product(zz, rr, store)
+        first(rr, zz, r).start()
+        return carry
+
+    lax.fori_loop(0, Z * (R - 1), phase1, 0)
+
+    def f_copy(q, zz, rr, slot):
+        return pltpu.make_async_remote_copy(
+            src_ref=f_ref, dst_ref=f_all.at[rows(slot, FR), :],
+            send_sem=fa_send.at[q], recv_sem=fa_recv.at[slot],
+            device_id=device(zz, rr, t), device_id_type=MESH,
+        )
+
+    def m_copy(src, dst, ss, rs, q, zz, rr, slot):
+        return pltpu.make_async_remote_copy(
+            src_ref=src.at[:, column(zz, rr)], dst_ref=dst.at[rows(slot, MR), :],
+            send_sem=ss.at[q], recv_sem=rs.at[slot],
+            device_id=device(zz, rr, t), device_id_type=MESH,
+        )
+
+    def spread(p, carry):
+        q, zz, rr = peer(p)
+        f_copy(q, zz, rr, me).start()
+        m_copy(m1_ref, m1_all, ma_send, ma_recv, q, zz, rr, me).start()
+        m_copy(m2_ref, m2_all, mb_send, mb_recv, q, zz, rr, me).start()
+        return carry
+
+    lax.fori_loop(1, N, spread, 0)
+    f_all[rows(me, FR), :] = f_ref[...]
+    m1_all[rows(me, MR), :] = m1_ref[:, column(z, r)]
+    m2_all[rows(me, MR), :] = m2_ref[:, column(z, r)]
+
+    def own_block(i, carry):
+        def store(part, value):
+            own[i, part, :] = value
+
+        product(i, r, store)
+        return carry
+
+    lax.fori_loop(0, Z, own_block, 0)
+
+    def join(zz, store):
+        def wait(d, carry):
+            src = lax.rem(r + d, R)
+            first(src, zz, src).wait_recv()
+            return carry
+
+        lax.fori_loop(1, R, wait, 0)
+
+        def tile(i, carry):
+            part = pl.ds(pl.multiple_of(i * TILE, TILE), TILE)
+            total = own[zz, part, :]
+            for d in range(1, R):
+                total = total + recv1[lax.rem(r + d, R), zz, part, :].astype(jnp.float32)
+            store(part, total)
+            return carry
+
+        lax.fori_loop(0, DH // TILE, tile, 0)
+
+    def phase2(e, carry):
+        zz = lax.rem(z + e, Z)
+
+        def store(part, value):
+            send2[zz, part, :] = value.astype(jnp.bfloat16)
+
+        join(zz, store)
+        second(zz, z).start()
+        return carry
+
+    lax.fori_loop(1, Z, phase2, 0)
+
+    def store_own(part, value):
+        grad[part, :] = value
+
+    join(z, store_own)
+
+    def wait_spread(p, carry):
+        q, zz, rr = peer(p)
+        f_copy(q, zz, rr, q).wait()
+        m_copy(m1_ref, m1_all, ma_send, ma_recv, q, zz, rr, q).wait()
+        m_copy(m2_ref, m2_all, mb_send, mb_recv, q, zz, rr, q).wait()
+        return carry
+
+    lax.fori_loop(1, N, wait_spread, 0)
+
+    def wait_second(e, carry):
+        src = lax.rem(z + e, Z)
+        second(src, src).wait_recv()
+        return carry
+
+    lax.fori_loop(1, Z, wait_second, 0)
+
+    def add_second(i, carry):
+        part = pl.ds(pl.multiple_of(i * TILE, TILE), TILE)
+        total = grad[part, :]
+        for e in range(1, Z):
+            total = total + recv2[lax.rem(z + e, Z), part, :].astype(jnp.float32)
+        grad[part, :] = total
+        return carry
+
+    lax.fori_loop(0, DH // TILE, add_second, 0)
+
+    projected = contract_rows(f_all[...], grad[...].astype(jnp.bfloat16))
+    new_first = 0.8 * m1_all[...] + 0.2 * projected
+    new_second = 0.9 * m2_all[...] + 0.1 * projected * projected
+    nf_col[...] = new_first
+    ns_col[...] = new_second
+    dir_low = (new_first / (jnp.sqrt(new_second) + 1e-08)).astype(jnp.bfloat16)
+    proj_low = projected.astype(jnp.bfloat16)
+    dir_wide = dir_low.astype(jnp.float32)
+    proj_wide = proj_low.astype(jnp.float32)
+    stat[0] = jnp.broadcast_to(jnp.sum(dir_wide * dir_wide, axis=0, keepdims=True), (8, LANES))
+    stat[1] = jnp.broadcast_to(jnp.sum(proj_wide * proj_wide, axis=0, keepdims=True), (8, LANES))
+    stat_all[every] = stat[...]
+
+    def s_copy(p, slot_of):
+        q = lax.rem(every + p, N * T)
+        d = q // T
+        slot = slot_of(q)
+        return pltpu.make_async_remote_copy(
+            src_ref=stat, dst_ref=stat_all.at[slot],
+            send_sem=st_send.at[q], recv_sem=st_recv.at[slot],
+            device_id=device(d // R, lax.rem(d, R), lax.rem(q, T)), device_id_type=MESH,
+        )
+
+    def send_stat(p, carry):
+        s_copy(p, lambda q: every).start()
+        return carry
+
+    lax.fori_loop(1, N * T, send_stat, 0)
+
+    def back_copy(src, dst, size, ss, rs, q, zz, rr, sz, sr, slot):
+        return pltpu.make_async_remote_copy(
+            src_ref=src.at[rows(q, size), :], dst_ref=dst.at[:, column(sz, sr)],
+            send_sem=ss.at[q], recv_sem=rs.at[slot],
+            device_id=device(zz, rr, t), device_id_type=MESH,
+        )
+
+    def send_moments(p, carry):
+        q, zz, rr = peer(p)
+        back_copy(nf_col, nf_ref, MR, nf_send, nf_recv, q, zz, rr, z, r, me).start()
+        back_copy(ns_col, ns_ref, MR, ns_send, ns_recv, q, zz, rr, z, r, me).start()
+        return carry
+
+    lax.fori_loop(1, N, send_moments, 0)
+    nf_ref[:, column(z, r)] = nf_col[rows(me, MR), :]
+    ns_ref[:, column(z, r)] = ns_col[rows(me, MR), :]
+
+    upd_col[...] = jnp.dot(f_all[...], dir_low, preferred_element_type=jnp.float32)
+    grad[...] = grad[...] - jnp.dot(f_all[...], proj_low, preferred_element_type=jnp.float32)
+
+    def wait_stat(p, carry):
+        s_copy(p, lambda q: q).wait()
+        return carry
+
+    lax.fori_loop(1, N * T, wait_stat, 0)
+    totals = jnp.sum(stat_all[...], axis=0)
+    dir_sum = jnp.sum(totals[0, 0:1, :], axis=1, keepdims=True)
+    proj_sum = jnp.sum(totals[1, 0:1, :], axis=1, keepdims=True)
+    scale_ratio = jnp.sqrt(dir_sum) / jnp.sqrt(proj_sum + 1e-06)
+    upd_col[...] = upd_col[...] + scale_ratio * grad[...]
+
+    def send_update(p, carry):
+        q, zz, rr = peer(p)
+        back_copy(upd_col, upd_ref, FR, up_send, up_recv, q, zz, rr, z, r, me).start()
+        return carry
+
+    lax.fori_loop(1, N, send_update, 0)
+    upd_ref[:, column(z, r)] = upd_col[rows(me, FR), :]
+
+    def wait_update(p, carry):
+        q, zz, rr = peer(p)
+        back_copy(upd_col, upd_ref, FR, up_send, up_recv, q, zz, rr, zz, rr, q).wait()
+        return carry
+
+    lax.fori_loop(1, N, wait_update, 0)
+
+    new_weight = w_ref[...] - 0.01 * upd_ref[...]
+    nw_ref[...] = new_weight
+    wc_ref[rows(me, FR), :] = new_weight.astype(jnp.bfloat16)
+
+    def along_z(zz, src):
+        block = wc_ref.at[rows(src * R + r, FR), :]
+        return pltpu.make_async_remote_copy(
+            src_ref=block, dst_ref=block, send_sem=gz_send.at[zz], recv_sem=gz_recv.at[src],
+            device_id=device(zz, r, t), device_id_type=MESH,
+        )
+
+    def along_r(rr, zz, src):
+        block = wc_ref.at[rows(zz * R + src, FR), :]
+        return pltpu.make_async_remote_copy(
+            src_ref=block, dst_ref=block, send_sem=gr_send.at[rr, zz], recv_sem=gr_recv.at[src, zz],
+            device_id=device(z, rr, t), device_id_type=MESH,
+        )
+
+    def start_z(e, carry):
+        along_z(lax.rem(z + e, Z), z).start()
+        return carry
+
+    lax.fori_loop(1, Z, start_z, 0)
+
+    def relay(e, carry):
+        zz = lax.rem(z + Z - e, Z)
+
+        @pl.when(e > 0)
+        def _():
+            along_z(zz, zz).wait_recv()
+
+        def start_r(d, carry):
+            along_r(lax.rem(r + d, R), zz, r).start()
+            return carry
+
+        return lax.fori_loop(1, R, start_r, carry)
+
+    lax.fori_loop(0, Z, relay, 0)
+
+    def drain(i, carry):
+        zz = i // (R - 1)
+        rr = lax.rem(r + 1 + lax.rem(i, R - 1), R)
+        along_r(rr, zz, rr).wait()
+        first(rr, zz, r).wait_send()
+        return carry
+
+    lax.fori_loop(0, Z * (R - 1), drain, 0)
+
+    def drain_z(e, carry):
+        zz = lax.rem(z + e, Z)
+        along_z(zz, z).wait_send()
+        second(zz, z).wait_send()
+        return carry
+
+    lax.fori_loop(1, Z, drain_z, 0)
+
+    def drain_moments(p, carry):
+        q, zz, rr = peer(p)
+        back_copy(nf_col, nf_ref, MR, nf_send, nf_recv, q, zz, rr, zz, rr, q).wait()
+        back_copy(ns_col, ns_ref, MR, ns_send, ns_recv, q, zz, rr, zz, rr, q).wait()
+        return carry
+
+    lax.fori_loop(1, N, drain_moments, 0)
+
+
+def fused(Z, R, T, *args):
+    mixer_out, out_grad, factors, weight, first_moment, second_moment = args
+    N = Z * R
+    DH = mixer_out.shape[1]
+    rank = factors.shape[1]
+    f32, bf16 = jnp.float32, jnp.bfloat16
+    vmem = pl.BlockSpec(memory_space=pltpu.VMEM)
+    dma = pltpu.SemaphoreType.DMA
+    wide = lambda n: [dma((n,)), dma((n,))]
+    return pl.pallas_call(
+        functools.partial(fused_kernel, Z, R, T),
+        out_shape=(
+            jax.ShapeDtypeStruct(weight.shape, f32),
+            jax.ShapeDtypeStruct(weight.shape, f32),
+            jax.ShapeDtypeStruct(first_moment.shape, f32),
+            jax.ShapeDtypeStruct(first_moment.shape, f32),
+            jax.ShapeDtypeStruct((DH, weight.shape[1]), bf16),
+        ),
+        in_specs=[vmem] * 6,
+        out_specs=(vmem,) * 5,
+        scratch_shapes=[
+            pltpu.VMEM((DH, mixer_out.shape[0]), bf16),
+            pltpu.VMEM((R, Z, DH, LANES), bf16),
+            pltpu.VMEM((R, Z, DH, LANES), bf16),
+            pltpu.VMEM((Z, DH, LANES), f32),
+            pltpu.VMEM((Z, DH, LANES), bf16),
+            pltpu.VMEM((Z, DH, LANES), bf16),
+            pltpu.VMEM((DH, LANES), f32),
+            pltpu.VMEM((DH, rank), bf16),
+            pltpu.VMEM((rank, LANES), f32),
+            pltpu.VMEM((rank, LANES), f32),
+            pltpu.VMEM((rank, LANES), f32),
+            pltpu.VMEM((rank, LANES), f32),
+            pltpu.VMEM((DH, LANES), f32),
+            pltpu.VMEM((2, 8, LANES), f32),
+            pltpu.VMEM((N * T, 2, 8, LANES), f32),
+            dma((R, Z)), dma((R, Z)), *wide(Z),
+            *wide(N), *wide(N), *wide(N),
+            *wide(N * T), *wide(N), *wide(N), *wide(N),
+            *wide(Z), dma((R, Z)), dma((R, Z)),
+        ],
+        compiler_params=pltpu.CompilerParams(
+            collective_id=0, has_side_effects=True, vmem_limit_bytes=60 * 1024 * 1024
+        ),
+    )(*args)
+
+def plain(mixer_out, out_grad, factors, weight, first_moment, second_moment):
     columns = mixer_out
     gradient = lax.psum_scatter(
         contract_rows(columns, out_grad), ("fs", "rep"), scatter_dimension=0, tiled=True
@@ -44,6 +423,19 @@
 
 
 def solution(mesh):
+    Z, R, T = mesh.shape["fs"], mesh.shape["rep"], mesh.shape["tp"]
+
+    def per_device(*args):
+        mixer_out, out_grad, factors, weight, first_moment, second_moment = args
+        fits = (
+            out_grad.shape[1] == Z * R * LANES
+            and mixer_out.shape[1] % TILE == 0
+            and weight.shape[0] % 16 == 0
+            and first_moment.shape[0] % 8 == 0
+            and min(Z, R) > 1
+        )
+        return fused(Z, R, T, *args) if fits else plain(*args)
+
     in_specs = (
         P(("fs", "rep"), None),
         P(("fs", "rep"), "tp"),

time: 534 us -> 222 us (0.42)
  waiting for transfers between devices: 433 us -> 0 us
  Pallas kernels: 0 us -> 207 us
  blocking collectives: 49.1 us -> 0 us
  matrix products: 20.1 us -> 0 us
  between operations: 15.2 us -> 0.64 us
    reduce_scatter x2 -> x0, waiting for transfers between devices: 274 us -> none  [the longest x1 203 us: per_device(): lax.psum_scatter(contract_rows(columns, out_grad), ('fs', 'rep'), scatter...]
    pallas_call x0 -> x1, Pallas kernels: none -> 207 us  [fused(): pl.pallas_call(functools.partial(fused_kernel, Z, R, T), out_shape=(jax.S...]
    all_gather x3 -> x0, waiting for transfers between devices: 158 us -> none  [the longest x1 93.6 us: per_device(): lax.all_gather(new_weight.astype(jnp.bfloat16), ('fs', 'rep'), axis=0, ti...]
    psum x1 -> x0, blocking collectives: 49.1 us -> none  [per_device(): lax.psum((jnp.sum(dir_wide * dir_wide), jnp.sum(proj_wide * proj_wide)),...]
    dot_general x4 -> x0, matrix products: 20.1 us -> none  [the longest x2 14.2 us: contract_rows(): lax.dot_general(left, right, (((0,), (0,)), ((), ())), preferred_element_...]
    unnamed x10 -> x5, local copies, waits for them, and re-layouts: 11.4 us -> 13.9 us
  transfers between devices with their start and end apart: 5 -> 0, of which waited for: 5 -> 0; matrix products, arithmetic and copies ran while one was open for 0% -> 0% of each run, Pallas kernels for 0% -> 0%
where the time goes in v1:
time: 222 us
  Pallas kernels  207 us (93%)
  local copies, waits for them, and re-layouts  13.9 us (6%)
    pallas_call x1, Pallas kernels, fused(): pl.pallas_call(functools.partial(fused_kernel, Z, R, T), out_shape=(jax.S...  207 us
    unnamed x5, local copies, waits for them, and re-layouts  13.9 us

profile of v1, /device:TPU:18, one launch (start us, length us, event | category | flops | bytes accessed | tf_op | source)
XLA Modules:
  0.0 221.7 jit_solution(2891099877090668094)
XLA Ops:
  0.6 207.2 %shard_map.101 = (f32[96,2048]{1,0:T(8,128)}, f32[96,2048]{1,0:T(8,128)}, f32[16,2048]{1,0:T(8,128)}, f32[16,2048]{1,0:T(8,128)}, bf16[1536,2048]{1,0:T(8,128)(2,1)}) custom-call(bf16[1024,1536]{1,0:T(8,128)(2,1)} %m_ref.1, bf16[1024,2048]{1,0:T(8,128)(2,1)} %o_ref.1, bf16[96,256]{1,0:T(8,128)(2,1)} %f_ref.1, f32[96,2048]{1,0:T(8,128)} %w_ref.1, ...), custom_call_target="tpu_custom_call" | custom-call | tf_op jit(solution)/shard_map/pallas_call | solution.py:355
  207.9 2.1 copy.16
  209.9 2.1 copy.17
  212.0 1.6 copy.18
  213.5 1.6 copy.19
  215.1 6.6 %copy.20 = bf16[1536,2048]{1,0:T(8,128)(2,1)} copy(bf16[1536,2048]{1,0:T(8,128)(2,1)} %get-tuple-element.14) | data formatting | bytes 12582912

commit v2 on v1

--- a/solution.py
+++ b/solution.py
@@ -28,6 +28,7 @@
     fa_send, fa_recv, ma_send, ma_recv, mb_send, mb_recv,
     st_send, st_recv, nf_send, nf_recv, ns_send, ns_recv, up_send, up_recv,
     gz_send, gz_recv, gr_send, gr_recv,
+    recvd, d_send, d_recv, gh_send, gh_recv,
 ):
     N = Z * R
     z, r, t = lax.axis_index("fs"), lax.axis_index("rep"), lax.axis_index("tp")
@@ -36,6 +37,8 @@
     DH = m_ref.shape[1]
     FR = f_ref.shape[0]
     MR = m1_ref.shape[0]
+    H, TH, FH = DH // 2, DH // TILE // 2, FR // 2
+    xn, yn, dn = r + 1 - 2 * lax.rem(r, 2), lax.rem(r + 2, R), R - 1 - r
 
     def device(zz, rr, tt):
         return {"fs": zz, "rep": rr, "tp": tt}
@@ -70,7 +73,7 @@
     lax.fori_loop(0, DH // TILE, turn, 0)
     pl.semaphore_wait(barrier, N * T - 1)
 
-    def product(zz, rr, store):
+    def product(zz, rr, store, lo=0, hi=None):
         cols = column(zz, rr)
 
         def tile(i, carry):
@@ -78,7 +81,7 @@
             store(part, jnp.dot(mt[part, :], o_ref[:, cols], preferred_element_type=jnp.float32))
             return carry
 
-        lax.fori_loop(0, DH // TILE, tile, 0)
+        lax.fori_loop(lo, DH // TILE if hi is None else hi, tile, 0)
 
     def first(rr, zz, src):
         return pltpu.make_async_remote_copy(
@@ -94,18 +97,45 @@
             device_id=device(zz, r, t), device_id_type=MESH,
         )
 
-    def phase1(i, carry):
-        zz = lax.rem(z + 1 + i // (R - 1), Z)
-        rr = lax.rem(r + 1 + lax.rem(i, R - 1), R)
+    def via(h, zz):
+        return pltpu.make_async_remote_copy(
+            src_ref=send1.at[dn, zz, pl.ds(h * H, H), :], dst_ref=recvd.at[h, zz],
+            send_sem=d_send.at[h, zz], recv_sem=d_recv.at[h, zz],
+            device_id=device(z, yn if h else xn, t), device_id_type=MESH,
+        )
+
+    def across(e, carry):
+        zz = lax.rem(z + 1 + e, Z)
 
         def store(part, value):
-            send1[rr, zz, part, :] = value.astype(jnp.bfloat16)
-
-        product(zz, rr, store)
-        first(rr, zz, r).start()
-        return carry
-
-    lax.fori_loop(0, Z * (R - 1), phase1, 0)
+            send1[dn, zz, part, :] = value.astype(jnp.bfloat16)
+
+        product(zz, dn, store)
+        via(0, zz).start()
+        via(1, zz).start()
+        return carry
+
+    lax.fori_loop(0, Z, across, 0)
+
+    def beside(e, carry):
+        zz = lax.rem(z + 1 + e, Z)
+        for h, rr in ((1, xn), (0, yn)):
+
+            def store(part, value):
+                send1[rr, zz, part, :] = value.astype(jnp.bfloat16)
+
+            def store_sum(part, value):
+                inner = pl.ds(pl.multiple_of(part.start - h * H, TILE), TILE)
+                total = value + recvd[h, zz, inner, :].astype(jnp.float32)
+                send1[rr, zz, part, :] = total.astype(jnp.bfloat16)
+
+            product(zz, rr, store, (1 - h) * TH, (2 - h) * TH)
+            via(h, zz).wait_recv()
+            product(zz, rr, store_sum, h * TH, (h + 1) * TH)
+            first(rr, zz, r).start()
+        return carry
+
+    lax.fori_loop(0, Z, beside, 0)
 
     def f_copy(q, zz, rr, slot):
         return pltpu.make_async_remote_copy(
@@ -143,18 +173,14 @@
     lax.fori_loop(0, Z, own_block, 0)
 
     def join(zz, store):
-        def wait(d, carry):
-            src = lax.rem(r + d, R)
+        for src in (xn, yn):
             first(src, zz, src).wait_recv()
-            return carry
-
-        lax.fori_loop(1, R, wait, 0)
 
         def tile(i, carry):
             part = pl.ds(pl.multiple_of(i * TILE, TILE), TILE)
             total = own[zz, part, :]
-            for d in range(1, R):
-                total = total + recv1[lax.rem(r + d, R), zz, part, :].astype(jnp.float32)
+            for src in (xn, yn):
+                total = total + recv1[src, zz, part, :].astype(jnp.float32)
             store(part, total)
             return carry
 
@@ -302,29 +328,47 @@
 
     lax.fori_loop(1, Z, start_z, 0)
 
+    def half(h, zz, src):
+        block = wc_ref.at[pl.ds(pl.multiple_of((zz * R + src) * FR + h * FH, FH), FH), :]
+        return pltpu.make_async_remote_copy(
+            src_ref=block, dst_ref=block, send_sem=gh_send.at[h, zz], recv_sem=gh_recv.at[h, zz],
+            device_id=device(z, xn if h else yn, t), device_id_type=MESH,
+        )
+
     def relay(e, carry):
-        zz = lax.rem(z + Z - e, Z)
+        zz = lax.rem(z + 2 * Z - e, Z)
+        last = lax.rem(z + 2 * Z - e + 1, Z)
+
+        @pl.when(e < Z)
+        def _():
+            @pl.when(e > 0)
+            def _():
+                along_z(zz, zz).wait_recv()
+
+            along_r(xn, zz, r).start()
+            along_r(yn, zz, r).start()
 
         @pl.when(e > 0)
         def _():
-            along_z(zz, zz).wait_recv()
-
-        def start_r(d, carry):
-            along_r(lax.rem(r + d, R), zz, r).start()
-            return carry
-
-        return lax.fori_loop(1, R, start_r, carry)
-
-    lax.fori_loop(0, Z, relay, 0)
-
-    def drain(i, carry):
-        zz = i // (R - 1)
-        rr = lax.rem(r + 1 + lax.rem(i, R - 1), R)
-        along_r(rr, zz, rr).wait()
-        first(rr, zz, r).wait_send()
-        return carry
-
-    lax.fori_loop(0, Z * (R - 1), drain, 0)
+            along_r(xn, last, xn).wait_recv()
+            half(0, last, xn).start()
+            along_r(yn, last, yn).wait_recv()
+            half(1, last, yn).start()
+
+        return carry
+
+    lax.fori_loop(0, Z + 1, relay, 0)
+
+    def drain(zz, carry):
+        for h, rr in ((0, xn), (1, yn)):
+            along_r(rr, zz, r).wait_send()
+            first(rr, zz, r).wait_send()
+            via(h, zz).wait_send()
+            half(h, zz, rr).wait_send()
+            half(h, zz, dn).wait_recv()
+        return carry
+
+    lax.fori_loop(0, Z, drain, 0)
 
     def drain_z(e, carry):
         zz = lax.rem(z + e, Z)
@@ -383,6 +427,8 @@
             *wide(N), *wide(N), *wide(N),
             *wide(N * T), *wide(N), *wide(N), *wide(N),
             *wide(Z), dma((R, Z)), dma((R, Z)),
+            pltpu.VMEM((2, Z, DH // 2, LANES), bf16),
+            dma((2, Z)), dma((2, Z)), dma((2, Z)), dma((2, Z)),
         ],
         compiler_params=pltpu.CompilerParams(
             collective_id=0, has_side_effects=True, vmem_limit_bytes=60 * 1024 * 1024
@@ -429,10 +475,11 @@
         mixer_out, out_grad, factors, weight, first_moment, second_moment = args
         fits = (
             out_grad.shape[1] == Z * R * LANES
-            and mixer_out.shape[1] % TILE == 0
-            and weight.shape[0] % 16 == 0
+            and mixer_out.shape[1] % (2 * TILE) == 0
+            and weight.shape[0] % 32 == 0
             and first_moment.shape[0] % 8 == 0
-            and min(Z, R) > 1
+            and R == 4
+            and Z > 1
         )
         return fused(Z, R, T, *args) if fits else plain(*args)
 

time: 222 us -> 215 us (0.968)
  Pallas kernels: 207 us -> 200 us
    pallas_call x1, Pallas kernels: 207 us -> 200 us  [fused(): pl.pallas_call(functools.partial(fused_kernel, Z, R, T), out_shape=(jax.S...]
where the time goes in v2:
time: 215 us
  Pallas kernels  200 us (93%)
  local copies, waits for them, and re-layouts  13.9 us (6%)
    pallas_call x1, Pallas kernels, fused(): pl.pallas_call(functools.partial(fused_kernel, Z, R, T), out_shape=(jax.S...  200 us
    unnamed x5, local copies, waits for them, and re-layouts  13.9 us

profile of v2, /device:TPU:18, one launch (start us, length us, event | category | flops | bytes accessed | tf_op | source)
XLA Modules:
  0.0 214.6 jit_solution(9630032758656842657)
XLA Ops:
  0.6 200.1 %shard_map.101 = (f32[96,2048]{1,0:T(8,128)}, f32[96,2048]{1,0:T(8,128)}, f32[16,2048]{1,0:T(8,128)}, f32[16,2048]{1,0:T(8,128)}, bf16[1536,2048]{1,0:T(8,128)(2,1)}) custom-call(bf16[1024,1536]{1,0:T(8,128)(2,1)} %m_ref.1, bf16[1024,2048]{1,0:T(8,128)(2,1)} %o_ref.1, bf16[96,256]{1,0:T(8,128)(2,1)} %f_ref.1, f32[96,2048]{1,0:T(8,128)} %w_ref.1, ...), custom_call_target="tpu_custom_call" | custom-call | tf_op jit(solution)/shard_map/pallas_call | solution.py:399
  200.7 2.1 copy.16
  202.8 2.1 copy.17
  204.8 1.6 copy.18
  206.4 1.6 copy.19
  208.0 6.6 %copy.20 = bf16[1536,2048]{1,0:T(8,128)(2,1)} copy(bf16[1536,2048]{1,0:T(8,128)(2,1)} %get-tuple-element.14) | data formatting | bytes 12582912
